TPU v7x, 32 devices: a whole 2x2x4 slice. The times are simulated.
32 devices in a mesh: kv: 4 (over y, x), tp: 8 (over z, core).
Axes of the slice: x: 2, y: 2, z: 4, core: 2. Of those that a mesh axis runs over, the one named last changes fastest.
Arguments:
- residual: bfloat16 [128, 4096], P(None, ('kv', 'tp')), may hold values from -20 to 20
- mixer_gain: float32 [4096], P('kv'), may hold values from 0.1 to 1.9
- w_query: bfloat16 [4096, 4096], P('kv', 'tp'), may hold values from -0.09375 to 0.09375
- w_forget: bfloat16 [4096, 4096], P('kv', 'tp'), may hold values from -0.09375 to 0.09375
- w_input: bfloat16 [4096, 4096], P('kv', 'tp'), may hold values from -0.09375 to 0.09375
- w_outgate: bfloat16 [4096, 4096], P('kv', 'tp'), may hold values from -0.09375 to 0.09375
- lower_bound: float32 [4096], P('tp'), may hold values from 0.3 to 0.97
- state: float32 [128, 32, 128, 128], P('kv', 'tp'), may hold values from -6 to 6
- head_gain: float32 [128], replicated, may hold values from 0.1 to 1.9
- w_mix_out: bfloat16 [4096, 4096], P('tp', 'kv'), may hold values from -0.09375 to 0.09375
- ffn_gain: float32 [4096], P('kv'), may hold values from 0.1 to 1.9
- w_gate: bfloat16 [4096, 10752], P('kv', 'tp'), may hold values from -0.09375 to 0.09375
- w_up: bfloat16 [4096, 10752], P('kv', 'tp'), may hold values from -0.09375 to 0.09375
- w_down: bfloat16 [10752, 4096], P('tp', 'kv'), may hold values from -0.0625 to 0.0625
Outputs:
- layer_out: bfloat16 [128, 4096], P(None, ('kv', 'tp'))
- new_state: float32 [128, 32, 128, 128], P('kv', 'tp')
All inputs are finite; a program needn't handle non-finite values.
Results may differ from a plain program's by a relative error of at most 0.015.
Values may be sent and summed in bfloat16 or wider, within the bound.
A program may use at most 64 MiB of HBM per device.

v0:
```python
import functools

import jax
import jax.numpy as jnp
from jax import lax
from jax.experimental import pallas as pl
from jax.experimental.pallas import tpu as pltpu
from jax.sharding import PartitionSpec as P

EPS = 1e-06
F32 = jnp.float32
BF16 = jnp.bfloat16
LANES = 128


def ring(axis, size):
    me = lax.axis_index(axis)
    return me, [lax.rem(me + step, size) for step in range(1, size)]


def greet(axes):
    barrier = pltpu.get_barrier_semaphore()
    count = 0
    for axis, peers in axes:
        for peer in peers:
            pl.semaphore_signal(
                barrier, inc=1, device_id={axis: peer}, device_id_type=pl.DeviceIdType.MESH
            )
            count += 1
    pl.semaphore_wait(barrier, count)


def remote(source, target, send_sem, recv_sem, axis, peer):
    return pltpu.make_async_remote_copy(
        src_ref=source,
        dst_ref=target,
        send_sem=send_sem,
        recv_sem=recv_sem,
        device_id={axis: peer},
        device_id_type=pl.DeviceIdType.MESH,
    )


def pairs(n_tp):
    me = lax.axis_index("tp")
    core = lax.rem(me, 2)
    return me, core, lax.div(me, 2), me + 1 - 2 * core, n_tp // 2


def gather_pairs(n_tp, source, blocks, send, recv):
    me, _, _, partner, half = pairs(n_tp)
    peers = [lax.rem(me + 2 * i, n_tp) for i in range(1, half)]
    origins = [lax.rem(me - 2 * i + n_tp, n_tp) for i in range(1, half)]
    direct = [
        remote(source, blocks.at[me], send.at[i], recv.at[i], "tp", peer)
        for i, peer in enumerate(peers)
    ]
    direct.append(
        remote(source, blocks.at[me], send.at[half - 1], recv.at[half - 1], "tp", partner)
    )
    for copy in direct:
        copy.start()
    blocks[pl.ds(me, 1)] = source[...][None]
    relays = []
    for i, origin in enumerate(origins):
        direct[i].wait_recv()
        relay = remote(
            blocks.at[origin], blocks.at[origin],
            send.at[half + i], recv.at[half + i], "tp", partner,
        )
        relay.start()
        relays.append(relay)
    direct[-1].wait_recv()
    for relay in relays:
        relay.wait_recv()
    return direct + relays


def scale_block(blocks, gain_ref, scaled, count, width):
    squares = None
    for j in range(count):
        rows = blocks[j].astype(F32)
        cols = slice(j * width, (j + 1) * width)
        scaled[:, cols] = (rows * gain_ref[:, cols]).astype(BF16)
        term = rows * rows
        squares = term if squares is None else squares + term
    total = jnp.sum(squares, axis=1, keepdims=True)
    return jnp.broadcast_to(total, (total.shape[0], LANES))


def project_kernel(
    n_kv, n_tp, features,
    x_ref, gain_ref, wq, wf, wi, wo,
    out_ref,
    weights, blocks, scaled, parts, landed, squares, squares_in,
    w_sem, x_send, x_recv, p_send, p_recv, s_send, s_recv,
):
    seqs, width = x_ref.shape
    local = out_ref.shape[1]
    loads = [
        pltpu.make_async_copy(source, weights.at[i], w_sem.at[i])
        for i, source in enumerate((wq, wf, wi, wo))
    ]
    for load in loads:
        load.start()
    kv, kv_peers = ring("kv", n_kv)
    tp, tp_peers = ring("tp", n_tp)
    near = pairs(n_tp)[3]
    greet((("kv", kv_peers), ("tp", [near] + tp_peers[1::2])))

    gathers = gather_pairs(n_tp, x_ref, blocks, x_send, x_recv)
    squares[...] = scale_block(blocks, gain_ref, scaled, n_tp, width)
    square_copies = [
        remote(
            squares.at[pl.ds(pl.multiple_of(peer * local, local), local), :],
            squares_in.at[i], s_send.at[i], s_recv.at[i], "kv", peer,
        )
        for i, peer in enumerate(kv_peers)
    ]
    for copy in square_copies:
        copy.start()
    for load in loads:
        load.wait()
    part_copies = []
    for p in range(4):
        parts[p] = jnp.dot(scaled[...], weights[p], preferred_element_type=F32).astype(BF16)
        for i, peer in enumerate(kv_peers):
            copy = remote(
                parts.at[p, pl.ds(pl.multiple_of(peer * local, local), local), :],
                landed.at[i, p], p_send.at[i, p], p_recv.at[i, p], "kv", peer,
            )
            copy.start()
            part_copies.append(copy)
    own = pl.ds(pl.multiple_of(kv * local, local), local)
    total = squares[own, :]
    for copy in square_copies:
        copy.wait_recv()
    for i in range(n_kv - 1):
        total = total + squares_in[i]
    inverse = lax.rsqrt(total[:, :1] / features + EPS)
    for copy in part_copies:
        copy.wait_recv()
    for p in range(4):
        value = parts[p, own, :].astype(F32)
        for i in range(n_kv - 1):
            value = value + landed[i, p].astype(F32)
        out_ref[p] = value * inverse
    for copy in gathers + square_copies + part_copies:
        copy.wait_send()


def split(value):
    high = value.astype(BF16).astype(F32)
    return high, value - high


def state_kernel(q_ref, f_ref, v_ref, g_ref, bound_ref, gain_ref, state_ref, new_ref, normed_ref, heads):
    rows, width = q_ref.shape[1:]
    bound = bound_ref[...]
    raw = f_ref[0]
    forget = split(bound + (1.0 - bound) * jax.nn.sigmoid(raw))
    keyvec = split((1.0 - bound) * jax.nn.sigmoid(-raw))
    query = split(q_ref[0] * jax.nn.sigmoid(q_ref[0]))
    values = split(v_ref[0])
    left = jnp.concatenate([*forget, *keyvec, keyvec[0], *query], axis=0).T.astype(BF16)
    one, nil = jnp.ones((rows, width), F32), jnp.zeros((rows, width), F32)
    right = jnp.concatenate(
        [
            jnp.concatenate([one, one, nil, nil, nil, nil, nil], axis=0),
            jnp.concatenate([nil, nil, values[0], values[0], values[1], nil, nil], axis=0),
            jnp.concatenate([nil, nil, nil, nil, nil, one, one], axis=0),
        ],
        axis=1,
    ).astype(BF16)
    owner = lax.rem(lax.broadcasted_iota(jnp.int32, right.shape, 0), rows)
    for s in range(rows):
        mask = jnp.where(owner == s, 1.0, 0.0).astype(BF16)
        wide = jnp.dot(left, right * mask, preferred_element_type=F32)
        new = wide[:, :width] * state_ref[s, 0] + wide[:, width : 2 * width]
        new_ref[s, 0] = new
        heads[s : s + 1, :] = jnp.sum(wide[:, 2 * width :] * new, axis=0, keepdims=True)
    head = heads[...]
    inverse = lax.rsqrt(jnp.mean(head * head, axis=1, keepdims=True) + EPS)
    gate = g_ref[0]
    normed_ref[...] = head * inverse * gain_ref[...] * (gate * jax.nn.sigmoid(gate))


def mix_kernel(
    n_kv, n_tp, features,
    normed_ref, x_ref, gain_ref, w_mix, w_gate, w_up, w_down,
    out_ref,
    mix_w, gate_w, down_w, normed16, heads, terms, terms_pair, terms_out, terms_in, mixed, blocks, scaled,
    squares, squares_in, parts, landed, hidden, hiddens, downs, downs_pair, downs_out, downs_in,
    w_sem, n_send, n_recv, t_send, t_recv, m_send, m_recv, s_send, s_recv,
    g_send, g_recv, h_send, h_recv, d_send, d_recv,
):
    seqs, width = x_ref.shape
    local = normed_ref.shape[0]
    units = gate_w.shape[1]
    loads = [
        pltpu.make_async_copy(source, target, w_sem.at[i])
        for i, (source, target) in enumerate(
            ((w_mix, mix_w), (w_gate, gate_w.at[0]), (w_up, gate_w.at[1]), (w_down, down_w))
        )
    ]
    for load in loads:
        load.start()
    normed16[...] = normed_ref[...].astype(BF16)
    kv, kv_peers = ring("kv", n_kv)
    tp, tp_peers = ring("tp", n_tp)
    own = pl.ds(pl.multiple_of(kv * local, local), local)
    near = pairs(n_tp)[3]
    greet((("kv", kv_peers), ("tp", [near] + tp_peers[1::2])))

    pending = []
    copies = [
        remote(normed16, heads.at[own, :], n_send.at[i], n_recv.at[i], "kv", peer)
        for i, peer in enumerate(kv_peers)
    ]
    for copy in copies:
        copy.start()
    pending += copies
    heads[own, :] = normed16[...]
    loads[0].wait()
    for copy in copies:
        copy.wait_recv()

    group = max(1, 256 // width)
    while n_tp % group:
        group -= 1

    me, core, chip, partner, half = pairs(n_tp)

    def reduce_pairs(base, left, weight, sums, pair_in, joined, sums_in, send, recv):
        for t in range(0, n_tp, group):
            part = jnp.dot(
                left[...], weight[:, t * width : (t + group) * width], preferred_element_type=F32
            ).astype(BF16)
            for j in range(group):
                sums[(t + j) % 2, (t + j) // 2] = part[:, j * width : (j + 1) * width]
        first = remote(sums.at[1 - core], pair_in, send.at[0], recv.at[0], "tp", partner)
        first.start()
        first.wait_recv()

        def pair_sum(place):
            mine = sums[pl.ds(core, 1), pl.ds(place, 1)][0, 0].astype(F32)
            return mine + pair_in[pl.ds(place, 1)][0].astype(F32)

        out = [first]
        for i in range(1, half):
            joined[i - 1] = pair_sum(lax.rem(chip + i, half)).astype(BF16)
            copy = remote(
                joined.at[i - 1], sums_in.at[i - 1], send.at[i], recv.at[i],
                "tp", lax.rem(me + 2 * i, n_tp),
            )
            copy.start()
            out.append(copy)
        total = base + pair_sum(chip)
        for i in range(1, half):
            out[i].wait_recv()
            total = total + sums_in[i - 1].astype(F32)
        pending.extend(out)
        return total.astype(BF16)

    mixed[...] = reduce_pairs(
        x_ref[...].astype(F32), heads, mix_w, terms, terms_pair, terms_out, terms_in, t_send, t_recv
    )

    pending += gather_pairs(n_tp, mixed, blocks, m_send, m_recv)
    squares[...] = scale_block(blocks, gain_ref, scaled, n_tp, width)
    square_copies = [
        remote(
            squares.at[pl.ds(pl.multiple_of(peer * local, local), local), :],
            squares_in.at[i], s_send.at[i], s_recv.at[i], "kv", peer,
        )
        for i, peer in enumerate(kv_peers)
    ]
    for copy in square_copies:
        copy.start()
    pending += square_copies

    copies = []
    step = min(512, units)
    for g in range(2):
        loads[1 + g].wait()
        for c in range(0, units, step):
            end = min(c + step, units)
            parts[g, :, c:end] = lax.dot_general(
                scaled[...], gate_w[g, c:end, :], (((1,), (1,)), ((), ())),
                preferred_element_type=F32,
            ).astype(BF16)
        for i, peer in enumerate(kv_peers):
            copy = remote(
                parts.at[g, pl.ds(pl.multiple_of(peer * local, local), local), :],
                landed.at[i, g], g_send.at[i, g], g_recv.at[i, g], "kv", peer,
            )
            copy.start()
            copies.append(copy)
    pending += copies
    for copy in square_copies:
        copy.wait_recv()
    total = squares[own, :]
    for i in range(n_kv - 1):
        total = total + squares_in[i]
    inverse = lax.rsqrt(total[:, :1] / features + EPS)
    for copy in copies:
        copy.wait_recv()
    sums = []
    for g in range(2):
        value = parts[g, own, :].astype(F32)
        for i in range(n_kv - 1):
            value = value + landed[i, g].astype(F32)
        sums.append(value * inverse)
    hidden[...] = (sums[0] * jax.nn.sigmoid(sums[0]) * sums[1]).astype(BF16)

    copies = [
        remote(hidden, hiddens.at[own, :], h_send.at[i], h_recv.at[i], "kv", peer)
        for i, peer in enumerate(kv_peers)
    ]
    for copy in copies:
        copy.start()
    pending += copies
    hiddens[own, :] = hidden[...]
    loads[3].wait()
    for copy in copies:
        copy.wait_recv()
    out_ref[...] = reduce_pairs(
        mixed[...].astype(F32), hiddens, down_w, downs, downs_pair, downs_out, downs_in, d_send, d_recv
    )
    for copy in pending:
        copy.wait_send()


def in_vmem():
    return pl.BlockSpec(memory_space=pltpu.VMEM)


def in_hbm():
    return pl.BlockSpec(memory_space=pl.ANY)


def body(
    n_kv, n_tp,
    residual, mixer_gain, w_query, w_forget, w_input, w_outgate, lower_bound, state,
    head_gain, w_mix_out, ffn_gain, w_gate, w_up, w_down,
):
    seqs, width = residual.shape
    depth, hid = w_query.shape
    local, heads, dk, dv = state.shape
    units = w_gate.shape[1]
    features = depth * n_kv
    half = n_tp // 2
    dma = pltpu.SemaphoreType.DMA

    raw = pl.pallas_call(
        functools.partial(project_kernel, n_kv, n_tp, features),
        out_shape=jax.ShapeDtypeStruct((4, local, hid), F32),
        in_specs=[in_vmem()] * 2 + [in_hbm()] * 4,
        out_specs=in_vmem(),
        scratch_shapes=[
            pltpu.VMEM((4, depth, hid), BF16),
            pltpu.VMEM((n_tp, seqs, width), BF16),
            pltpu.VMEM((seqs, depth), BF16),
            pltpu.VMEM((4, seqs, hid), BF16),
            pltpu.VMEM((n_kv - 1, 4, local, hid), BF16),
            pltpu.VMEM((seqs, LANES), F32),
            pltpu.VMEM((n_kv - 1, local, LANES), F32),
            dma((4,)),
            dma((n_tp - 1,)), dma((n_tp - 1,)),
            dma((n_kv - 1, 4)), dma((n_kv - 1, 4)),
            dma((n_kv - 1,)), dma((n_kv - 1,)),
        ],
        compiler_params=pltpu.CompilerParams(collective_id=0, has_side_effects=True),
        name="project",
    )(residual, mixer_gain.reshape(1, depth), w_query, w_forget, w_input, w_outgate)

    rows = 16 if local % 16 == 0 else local
    pick = lambda p: pl.BlockSpec((1, rows, dk), lambda h, s: (p, s, h))
    updated, normed = pl.pallas_call(
        state_kernel,
        grid=(heads, local // rows),
        out_shape=(
            jax.ShapeDtypeStruct(state.shape, F32),
            jax.ShapeDtypeStruct((local, heads * dv), F32),
        ),
        in_specs=[
            pick(0), pick(1), pick(2), pick(3),
            pl.BlockSpec((1, dk), lambda h, s: (0, h)),
            pl.BlockSpec((1, dv), lambda h, s: (0, 0)),
            pl.BlockSpec((rows, 1, dk, dv), lambda h, s: (s, h, 0, 0)),
        ],
        out_specs=(
            pl.BlockSpec((rows, 1, dk, dv), lambda h, s: (s, h, 0, 0)),
            pl.BlockSpec((rows, dv), lambda h, s: (s, h)),
        ),
        scratch_shapes=[pltpu.VMEM((rows, dv), F32)],
        name="state",
    )(raw, raw, raw, raw, lower_bound.reshape(1, hid), head_gain.reshape(1, dv), state)

    layer_out = pl.pallas_call(
        functools.partial(mix_kernel, n_kv, n_tp, features),
        out_shape=jax.ShapeDtypeStruct((seqs, width), BF16),
        in_specs=[in_vmem()] * 3 + [in_hbm()] * 4,
        out_specs=in_vmem(),
        scratch_shapes=[
            pltpu.VMEM(w_mix_out.shape, BF16),
            pltpu.VMEM((2, units, depth), BF16),
            pltpu.VMEM(w_down.shape, BF16),
            pltpu.VMEM((local, hid), BF16),
            pltpu.VMEM((seqs, hid), BF16),
            pltpu.VMEM((2, half, seqs, width), BF16),
            pltpu.VMEM((half, seqs, width), BF16),
            pltpu.VMEM((half - 1, seqs, width), BF16),
            pltpu.VMEM((half - 1, seqs, width), BF16),
            pltpu.VMEM((seqs, width), BF16),
            pltpu.VMEM((n_tp, seqs, width), BF16),
            pltpu.VMEM((seqs, depth), BF16),
            pltpu.VMEM((seqs, LANES), F32),
            pltpu.VMEM((n_kv - 1, local, LANES), F32),
            pltpu.VMEM((2, seqs, units), BF16),
            pltpu.VMEM((n_kv - 1, 2, local, units), BF16),
            pltpu.VMEM((local, units), BF16),
            pltpu.VMEM((seqs, units), BF16),
            pltpu.VMEM((2, half, seqs, width), BF16),
            pltpu.VMEM((half, seqs, width), BF16),
            pltpu.VMEM((half - 1, seqs, width), BF16),
            pltpu.VMEM((half - 1, seqs, width), BF16),
            dma((4,)),
            dma((n_kv - 1,)), dma((n_kv - 1,)),
            dma((n_tp - 1,)), dma((n_tp - 1,)),
            dma((n_tp - 1,)), dma((n_tp - 1,)),
            dma((n_kv - 1,)), dma((n_kv - 1,)),
            dma((n_kv - 1, 2)), dma((n_kv - 1, 2)),
            dma((n_kv - 1,)), dma((n_kv - 1,)),
            dma((n_tp - 1,)), dma((n_tp - 1,)),
        ],
        compiler_params=pltpu.CompilerParams(collective_id=1, has_side_effects=True),
        name="mix",
    )(normed, residual, ffn_gain.reshape(1, depth), w_mix_out, w_gate.T, w_up.T, w_down)
    return layer_out, updated


def solution(mesh):
    in_specs = (
        P(None, ("kv", "tp")),
        P("kv"),
        P("kv", "tp"),
        P("kv", "tp"),
        P("kv", "tp"),
        P("kv", "tp"),
        P("tp"),
        P("kv", "tp", None, None),
        P(),
        P("tp", "kv"),
        P("kv"),
        P("kv", "tp"),
        P("kv", "tp"),
        P("tp", "kv"),
    )
    out_specs = (P(None, ("kv", "tp")), P("kv", "tp", None, None))
    return jax.shard_map(
        functools.partial(body, mesh.shape["kv"], mesh.shape["tp"]),
        mesh=mesh, in_specs=in_specs, out_specs=out_specs, check_vma=False,
    )
```

profile of v0, /device:TPU:0, one launch (start us, length us, event | category | flops | bytes accessed | tf_op | source)
XLA Modules:
  0.0 76.8 jit_solution(13784595635102939860)
XLA Ops:
  0.6 19.7 %project.1.q_ref.f_ref.v_ref.g_ref = f32[4,32,512]{2,1,0:T(8,128)} custom-call(bf16[128,128]{1,0:T(8,128)(2,1)} %x_ref.3, f32[1,1024]{1,0:T(1,128)} %bitcast.8, bf16[1024,512]{1,0:T(8,128)(2,1)} %wq.1, bf16[1024,512]{1,0:T(8,128)(2,1)} %wf.1, bf16[1024,512]{1,0:T(8,128)(2,1)} %wi.1, bf16[1024,512]{1,0:T(8,128)(2,1)} %wo.1), custom_call_target="tpu_custom_call" | custom-call | tf_op jit(solution)/shard_map/project/pallas_call | solution.py:355
  20.4 11.4 %state.1 = (f32[32,4,128,128]{3,2,1,0:T(8,128)}, f32[32,512]{1,0:T(8,128)}) custom-call(f32[4,32,512]{2,1,0:T(8,128)} %project.1.q_ref.f_ref.v_ref.g_ref, f32[4,32,512]{2,1,0:T(8,128)} %project.1.q_ref.f_ref.v_ref.g_ref, f32[4,32,512]{2,1,0:T(8,128)} %project.1.q_ref.f_ref.v_ref.g_ref, f32[4,32,512]{2,1,0:T(8,128)} %project.1.q_ref.f_ref.v_ref.g_ref, ...), custom_call_target="tpu_custom_call" | custom-call | tf_op jit(solution)/shard_map/state/pallas_call | solution.py:379
  31.8 43.6 %mix.1 = bf16[128,128]{1,0:T(8,128)(2,1)} custom-call(f32[32,512]{1,0:T(8,128)} %get-tuple-element.4.normed_ref, bf16[128,128]{1,0:T(8,128)(2,1)} %x_ref.3, f32[1,1024]{1,0:T(1,128)} %bitcast.9, bf16[512,1024]{1,0:T(8,128)(2,1)} %w_mix.1, bf16[1344,1024]{1,0:T(8,128)(2,1)} %bitcast.6, bf16[1344,1024]{1,0:T(8,128)(2,1)} %bitcast.7, bf16[1344,1024]{1,0:T(8,128)(2,1)} %w_down.1), custom_call_target="tpu_custom_call" | custom-call | tf_op jit(solution)/shard_map/mix/pallas_call | solution.py:400
  75.4 1.4 %copy.17 = bf16[128,128]{1,0:T(8,128)(2,1)} copy(bf16[128,128]{1,0:T(8,128)(2,1)} %mix.1) | data formatting | bytes 65536
where the time goes:
time: 77.3 us; the launch traced here: 76.8 us
  Pallas kernels  74.7 us (97%)
  local copies, waits for them, and re-layouts  1.38 us (2%)
    pallas_call x1, Pallas kernels, body(): pl.pallas_call(functools.partial(mix_kernel, n_kv, n_tp, features), out_s...  43.6 us
    pallas_call x1, Pallas kernels, body(): pl.pallas_call(functools.partial(project_kernel, n_kv, n_tp, features), o...  19.7 us
    pallas_call x1, Pallas kernels, body(): pl.pallas_call(state_kernel, grid=(heads, local // rows), out_shape=(jax....  11.4 us

commit v1 on v0

v1 whole, which is shorter than its diff:
```python
import functools

import jax
import jax.numpy as jnp
from jax import lax
from jax.experimental import pallas as pl
from jax.experimental.pallas import tpu as pltpu
from jax.sharding import PartitionSpec as P

EPS = 1e-06
F32 = jnp.float32
BF16 = jnp.bfloat16
LANES = 128


def ring(axis, size):
    me = lax.axis_index(axis)
    return me, [lax.rem(me + step, size) for step in range(1, size)]


def greet(axes):
    barrier = pltpu.get_barrier_semaphore()
    count = 0
    for axis, peers in axes:
        for peer in peers:
            pl.semaphore_signal(
                barrier, inc=1, device_id={axis: peer}, device_id_type=pl.DeviceIdType.MESH
            )
            count += 1
    pl.semaphore_wait(barrier, count)


def remote(source, target, send_sem, recv_sem, axis, peer):
    return pltpu.make_async_remote_copy(
        src_ref=source,
        dst_ref=target,
        send_sem=send_sem,
        recv_sem=recv_sem,
        device_id={axis: peer},
        device_id_type=pl.DeviceIdType.MESH,
    )


def pairs(n_tp):
    me = lax.axis_index("tp")
    core = lax.rem(me, 2)
    return me, core, lax.div(me, 2), me + 1 - 2 * core, n_tp // 2


def start_gather(n_tp, source, blocks, send, recv):
    me, _, _, partner, half = pairs(n_tp)
    targets = [lax.rem(me + 2 * i, n_tp) for i in range(1, half)] + [partner]
    direct = [
        remote(source, blocks.at[me], send.at[i], recv.at[i], "tp", target)
        for i, target in enumerate(targets)
    ]
    for copy in direct:
        copy.start()
    blocks[pl.ds(me, 1)] = source[...][None]
    return direct


def relay_gather(n_tp, blocks, direct, send, recv):
    me, _, _, partner, half = pairs(n_tp)
    relays = []
    for i in range(1, half):
        origin = lax.rem(me - 2 * i + n_tp, n_tp)
        direct[i - 1].wait_recv()
        relay = remote(
            blocks.at[origin], blocks.at[origin],
            send.at[half + i - 1], recv.at[half + i - 1], "tp", partner,
        )
        relay.start()
        relays.append(relay)
    return relays


def end_gather(direct, relays):
    direct[-1].wait_recv()
    for relay in relays:
        relay.wait_recv()


def scale_block(blocks, gain_ref, scaled, count, width):
    squares = None
    for j in range(count):
        rows = blocks[j].astype(F32)
        cols = slice(j * width, (j + 1) * width)
        scaled[:, cols] = (rows * gain_ref[:, cols]).astype(BF16)
        term = rows * rows
        squares = term if squares is None else squares + term
    total = jnp.sum(squares, axis=1, keepdims=True)
    return jnp.broadcast_to(total, (total.shape[0], LANES))


def layer_kernel(
    n_kv, n_tp, features, parts_of,
    x_hbm, gain_a_hbm, gain_b_hbm, bound_hbm, head_gain_hbm,
    wq, wf, wi, wo, state_hbm, w_mix, w_gate, w_up, w_down,
    out_ref, fkv_ref,
    xs, gain_a, gain_b, bound, head_gain, proj_w, state, mix_w, gate_w, down_w,
    blocks, scaled, squares, squares_in, raws, raws_in, normed, heads_all,
    sums, pair_in, joined, sums_in, mixed,
    parts, parts_in, hidden, hiddens,
    x_sem, small_sem, proj_sem, state_sem, w_sem,
    g_send, g_recv, q_send, q_recv, r_send, r_recv, n_send, n_recv,
    t_send, t_recv, p_send, p_recv, h_send, h_recv,
):
    halves = range(parts_of)
    _, seqs, width = xs.shape
    rows = seqs // n_kv
    n_heads, depth, wide = proj_w.shape
    dk = wide // 4
    units = gate_w.shape[1]
    half = n_tp // 2

    x_loads = []
    for h in halves:
        for o in range(n_kv):
            x_loads.append(pltpu.make_async_copy(
                x_hbm.at[pl.ds((o * parts_of + h) * rows, rows), :],
                xs.at[h, pl.ds(o * rows, rows), :], x_sem.at[h, o],
            ))
    small_loads = [
        pltpu.make_async_copy(source, target, small_sem.at[i])
        for i, (source, target) in enumerate((
            (gain_a_hbm, gain_a), (gain_b_hbm, gain_b), (bound_hbm, bound), (head_gain_hbm, head_gain),
        ))
    ]
    proj_loads = [
        [
            pltpu.make_async_copy(
                source.at[:, pl.ds(j * dk, dk)], proj_w.at[j, :, pl.ds(p * dk, dk)], proj_sem.at[j, p]
            )
            for p, source in enumerate((wq, wf, wi, wo))
        ]
        for j in range(n_heads)
    ]
    state_loads = [
        pltpu.make_async_copy(
            state_hbm.at[pl.ds(h * rows, rows)], state.at[pl.ds(h * rows, rows)], state_sem.at[h]
        )
        for h in halves
    ]
    w_loads = [
        pltpu.make_async_copy(source, target, w_sem.at[i])
        for i, (source, target) in enumerate(
            ((w_mix, mix_w), (w_gate, gate_w.at[0]), (w_up, gate_w.at[1]), (w_down, down_w))
        )
    ]
    for load in x_loads + small_loads + sum(proj_loads, []) + state_loads + w_loads:
        load.start()

    kv, kv_peers = ring("kv", n_kv)
    me, core, chip, partner, _ = pairs(n_tp)
    own = pl.ds(pl.multiple_of(kv * rows, rows), rows)
    peer_rows = [pl.ds(pl.multiple_of(peer * rows, rows), rows) for peer in kv_peers]
    tp_peers = ring("tp", n_tp)[1]
    greet((("kv", kv_peers), ("tp", [partner] + tp_peers[1::2])))

    pending = []

    def send_squares(h, stage):
        copies = [
            remote(
                squares.at[stage, h, peer_rows[i], :], squares_in.at[stage, h, i],
                q_send.at[stage, h, i], q_recv.at[stage, h, i], "kv", peer,
            )
            for i, peer in enumerate(kv_peers)
        ]
        for copy in copies:
            copy.start()
        pending.extend(copies)
        return copies

    def inverse_of(h, stage, copies):
        total = squares[stage, h, own, :]
        for i, copy in enumerate(copies):
            copy.wait_recv()
            total = total + squares_in[stage, h, i]
        return lax.rsqrt(total[:, :1] / features + EPS)

    def spread(h, stage, source, target, send, recv):
        copies = [
            remote(source, target.at[h, own, :], send.at[h, i], recv.at[h, i], "kv", peer)
            for i, peer in enumerate(kv_peers)
        ]
        for copy in copies:
            copy.start()
        pending.extend(copies)
        target[h, own, :] = source[...]
        return copies

    group = max(1, 256 // width)
    while n_tp % group:
        group -= 1

    def start_reduce(h, stage, left, weight):
        for t in range(0, n_tp, group):
            part = jnp.dot(
                left[...], weight[:, t * width : (t + group) * width], preferred_element_type=F32
            ).astype(BF16)
            for j in range(group):
                sums[stage, h, (t + j) % 2, (t + j) // 2] = part[:, j * width : (j + 1) * width]
        first = remote(
            sums.at[stage, h, 1 - core], pair_in.at[stage, h],
            t_send.at[stage, h, 0], t_recv.at[stage, h, 0], "tp", partner,
        )
        first.start()
        pending.append(first)
        return first

    def pair_sum(h, stage, place):
        mine = sums[stage, h, pl.ds(core, 1), pl.ds(place, 1)][0, 0].astype(F32)
        return mine + pair_in[stage, h, pl.ds(place, 1)][0].astype(F32)

    def join_reduce(h, stage, first):
        first.wait_recv()
        out = []
        for i in range(1, half):
            joined[stage, h, i - 1] = pair_sum(h, stage, lax.rem(chip + i, half)).astype(BF16)
            copy = remote(
                joined.at[stage, h, i - 1], sums_in.at[stage, h, i - 1],
                t_send.at[stage, h, i], t_recv.at[stage, h, i], "tp", lax.rem(me + 2 * i, n_tp),
            )
            copy.start()
            out.append(copy)
        pending.extend(out)
        return out

    def end_reduce(h, stage, base, out):
        total = base + pair_sum(h, stage, chip)
        for i, copy in enumerate(out):
            copy.wait_recv()
            total = total + sums_in[stage, h, i].astype(F32)
        return total.astype(BF16)

    direct, relays, square_copies, copies = {}, {}, {}, {}

    for h in halves:
        for load in x_loads[h * n_kv : (h + 1) * n_kv]:
            load.wait()
        direct[h] = start_gather(n_tp, xs.at[h], blocks.at[0, h], g_send.at[0, h], g_recv.at[0, h])
        pending += direct[h]
    for load in small_loads:
        load.wait()
    for h in halves:
        relays[h] = relay_gather(n_tp, blocks.at[0, h], direct[h], g_send.at[0, h], g_recv.at[0, h])
        pending += relays[h]
    for h in halves:
        end_gather(direct[h], relays[h])
        squares[0, h] = scale_block(blocks.at[0, h], gain_a, scaled.at[0, h], n_tp, width)
        square_copies[h] = send_squares(h, 0)
        copies[h] = []
        for j in range(n_heads):
            if h == 0:
                for load in proj_loads[j]:
                    load.wait()
            raws[h, j] = jnp.dot(scaled[0, h], proj_w[j], preferred_element_type=F32).astype(BF16)
            sent = [
                remote(
                    raws.at[h, j, peer_rows[i], :], raws_in.at[h, i, j],
                    r_send.at[h, i, j], r_recv.at[h, i, j], "kv", peer,
                )
                for i, peer in enumerate(kv_peers)
            ]
            for copy in sent:
                copy.start()
            copies[h].append(sent)
            pending += sent

    spots = lax.broadcasted_iota(jnp.int32, (rows, dk), 0)
    for h in halves:
        inverse = inverse_of(h, 0, square_copies[h])
        state_loads[h].wait()
        for j in range(n_heads):
            cols = slice(j * dk, (j + 1) * dk)
            total = raws[h, j, own, :].astype(F32)
            for i, copy in enumerate(copies[h][j]):
                copy.wait_recv()
                total = total + raws_in[h, i, j].astype(F32)
            total = total * inverse
            query, raw, value, gate = (total[:, p * dk : (p + 1) * dk] for p in range(4))
            low = bound[:, cols]
            forget = low + (1.0 - low) * jax.nn.sigmoid(raw)
            keyvec = (1.0 - low) * jax.nn.sigmoid(-raw)
            query = query * jax.nn.sigmoid(query)
            fkv_ref[0, h, j] = forget
            fkv_ref[1, h, j] = keyvec
            fkv_ref[2, h, j] = value
            left = (query * forget).astype(BF16)
            head = jnp.sum(query * keyvec, axis=1, keepdims=True) * value
            for s in range(rows):
                seen = jnp.dot(left, state[h * rows + s, j].astype(BF16), preferred_element_type=F32)
                head = head + jnp.where(spots == s, seen, 0.0)
            scale = lax.rsqrt(jnp.mean(head * head, axis=1, keepdims=True) + EPS)
            normed[h, :, cols] = (
                head * scale * head_gain[...] * (gate * jax.nn.sigmoid(gate))
            ).astype(BF16)
        copies[h] = spread(h, 0, normed.at[h], heads_all, n_send, n_recv)

    firsts, outs = {}, {}
    w_loads[0].wait()
    for h in halves:
        for copy in copies[h]:
            copy.wait_recv()
        firsts[h] = start_reduce(h, 0, heads_all.at[h], mix_w)
    for h in halves:
        outs[h] = join_reduce(h, 0, firsts[h])
    for h in halves:
        mixed[h] = end_reduce(h, 0, xs[h].astype(F32), outs[h])
        direct[h] = start_gather(n_tp, mixed.at[h], blocks.at[1, h], g_send.at[1, h], g_recv.at[1, h])
        pending += direct[h]
    for h in halves:
        relays[h] = relay_gather(n_tp, blocks.at[1, h], direct[h], g_send.at[1, h], g_recv.at[1, h])
        pending += relays[h]
    step = min(512, units)
    for h in halves:
        end_gather(direct[h], relays[h])
        squares[1, h] = scale_block(blocks.at[1, h], gain_b, scaled.at[1, h], n_tp, width)
        square_copies[h] = send_squares(h, 1)
        copies[h] = []
        for g in range(2):
            if h == 0:
                w_loads[1 + g].wait()
            for c in range(0, units, step):
                end = min(c + step, units)
                parts[h, g, :, c:end] = lax.dot_general(
                    scaled[1, h], gate_w[g, c:end, :], (((1,), (1,)), ((), ())),
                    preferred_element_type=F32,
                ).astype(BF16)
            sent = [
                remote(
                    parts.at[h, g, peer_rows[i], :], parts_in.at[h, i, g],
                    p_send.at[h, i, g], p_recv.at[h, i, g], "kv", peer,
                )
                for i, peer in enumerate(kv_peers)
            ]
            for copy in sent:
                copy.start()
            copies[h].append(sent)
            pending += sent
    for h in halves:
        inverse = inverse_of(h, 1, square_copies[h])
        both = []
        for g in range(2):
            total = parts[h, g, own, :].astype(F32)
            for i, copy in enumerate(copies[h][g]):
                copy.wait_recv()
                total = total + parts_in[h, i, g].astype(F32)
            both.append(total * inverse)
        hidden[h] = (both[0] * jax.nn.sigmoid(both[0]) * both[1]).astype(BF16)
        copies[h] = spread(h, 1, hidden.at[h], hiddens, h_send, h_recv)
    w_loads[3].wait()
    for h in halves:
        for copy in copies[h]:
            copy.wait_recv()
        firsts[h] = start_reduce(h, 1, hiddens.at[h], down_w)
    for h in halves:
        outs[h] = join_reduce(h, 1, firsts[h])
    for h in halves:
        out_ref[h] = end_reduce(h, 1, mixed[h].astype(F32), outs[h])
    for copy in pending:
        copy.wait_send()


def split(value):
    high = value.astype(BF16).astype(F32)
    return high, value - high


def update_kernel(parts_of, n_kv, fkv_ref, state_ref, part_ref, new_ref, out_ref, news, picks, sems):
    _, _, n_heads, rows, dk = fkv_ref.shape
    for h in range(parts_of):
        for o in range(n_kv):
            out_ref[pl.ds((o * parts_of + h) * rows, rows), :] = part_ref[h, pl.ds(o * rows, rows), :]
    place = lax.broadcasted_iota(jnp.int32, (4 * rows, 2 * dk), 0)
    lane = lax.broadcasted_iota(jnp.int32, (4 * rows, 2 * dk), 1)
    side = jnp.where((place < 2 * rows) == (lane < dk), 1.0, 0.0)
    owner = lax.rem(place, rows)
    for s in range(rows):
        picks[s] = jnp.where(owner == s, side, 0.0).astype(BF16)

    def chunk(h, j):
        at = (pl.ds(h * rows, rows), pl.ds(j, 1))
        return pltpu.make_async_copy(news.at[at], new_ref.at[at], sems.at[h, j])

    for h in range(parts_of):
        def step(j, carry, h=h):
            left = jnp.concatenate(
                [*split(fkv_ref[0, h, j]), *split(fkv_ref[1, h, j])], axis=0
            ).T.astype(BF16)
            value = fkv_ref[2, h, j]
            for s in range(rows):
                wide = jnp.dot(left, picks[s], preferred_element_type=F32)
                news[h * rows + s, j] = (
                    wide[:, :dk] * state_ref[h * rows + s, j] + wide[:, dk:] * value[s : s + 1, :]
                )
            chunk(h, j).start()
            return carry
        lax.fori_loop(0, n_heads, step, 0)
    for h in range(parts_of):
        for j in range(n_heads):
            chunk(h, j).wait()


def in_vmem():
    return pl.BlockSpec(memory_space=pltpu.VMEM)


def in_hbm():
    return pl.BlockSpec(memory_space=pltpu.HBM)


def body(
    n_kv, n_tp,
    residual, mixer_gain, w_query, w_forget, w_input, w_outgate, lower_bound, state,
    head_gain, w_mix_out, ffn_gain, w_gate, w_up, w_down,
):
    seqs, width = residual.shape
    depth, hid = w_query.shape
    local, n_heads, dk, dv = state.shape
    units = w_gate.shape[1]
    features = depth * n_kv
    half = n_tp // 2
    parts_of = 2 if local % 32 == 0 else 1
    rows = local // parts_of
    some = seqs // parts_of
    dma = pltpu.SemaphoreType.DMA
    stay = lambda array: pltpu.with_memory_space_constraint(array, pltpu.HBM)
    held = pltpu.with_memory_space_constraint(state, pltpu.VMEM)

    part, fkv = pl.pallas_call(
        functools.partial(layer_kernel, n_kv, n_tp, features, parts_of),
        out_shape=(
            jax.ShapeDtypeStruct((parts_of, some, width), BF16),
            jax.ShapeDtypeStruct((3, parts_of, n_heads, rows, dk), F32),
        ),
        in_specs=[in_hbm()] * 14,
        out_specs=(in_vmem(), in_vmem()),
        scratch_shapes=[
            pltpu.VMEM((parts_of, some, width), BF16),
            pltpu.VMEM((1, depth), F32),
            pltpu.VMEM((1, depth), F32),
            pltpu.VMEM((1, hid), F32),
            pltpu.VMEM((1, dv), F32),
            pltpu.VMEM((n_heads, depth, 4 * dk), BF16),
            pltpu.VMEM(state.shape, F32),
            pltpu.VMEM(w_mix_out.shape, BF16),
            pltpu.VMEM((2, units, depth), BF16),
            pltpu.VMEM(w_down.shape, BF16),
            pltpu.VMEM((2, parts_of, n_tp, some, width), BF16),
            pltpu.VMEM((2, parts_of, some, depth), BF16),
            pltpu.VMEM((2, parts_of, some, LANES), F32),
            pltpu.VMEM((2, parts_of, n_kv - 1, rows, LANES), F32),
            pltpu.VMEM((parts_of, n_heads, some, 4 * dk), BF16),
            pltpu.VMEM((parts_of, n_kv - 1, n_heads, rows, 4 * dk), BF16),
            pltpu.VMEM((parts_of, rows, hid), BF16),
            pltpu.VMEM((parts_of, some, hid), BF16),
            pltpu.VMEM((2, parts_of, 2, half, some, width), BF16),
            pltpu.VMEM((2, parts_of, half, some, width), BF16),
            pltpu.VMEM((2, parts_of, half - 1, some, width), BF16),
            pltpu.VMEM((2, parts_of, half - 1, some, width), BF16),
            pltpu.VMEM((parts_of, some, width), BF16),
            pltpu.VMEM((parts_of, 2, some, units), BF16),
            pltpu.VMEM((parts_of, n_kv - 1, 2, rows, units), BF16),
            pltpu.VMEM((parts_of, rows, units), BF16),
            pltpu.VMEM((parts_of, some, units), BF16),
            dma((parts_of, n_kv)), dma((4,)), dma((n_heads, 4)), dma((parts_of,)), dma((4,)),
            dma((2, parts_of, n_tp - 1)), dma((2, parts_of, n_tp - 1)),
            dma((2, parts_of, n_kv - 1)), dma((2, parts_of, n_kv - 1)),
            dma((parts_of, n_kv - 1, n_heads)), dma((parts_of, n_kv - 1, n_heads)),
            dma((parts_of, n_kv - 1)), dma((parts_of, n_kv - 1)),
            dma((2, parts_of, half)), dma((2, parts_of, half)),
            dma((parts_of, n_kv - 1, 2)), dma((parts_of, n_kv - 1, 2)),
            dma((parts_of, n_kv - 1)), dma((parts_of, n_kv - 1)),
        ],
        compiler_params=pltpu.CompilerParams(
            collective_id=0, has_side_effects=True, vmem_limit_bytes=44 * 2**20
        ),
        name="layer",
    )(*map(stay, (
        residual, mixer_gain.reshape(1, depth), ffn_gain.reshape(1, depth),
        lower_bound.reshape(1, hid), head_gain.reshape(1, dv),
        w_query, w_forget, w_input, w_outgate, state, w_mix_out, w_gate.T, w_up.T, w_down,
    )))

    updated, layer_out = pl.pallas_call(
        functools.partial(update_kernel, parts_of, n_kv),
        out_shape=(
            jax.ShapeDtypeStruct(state.shape, F32),
            jax.ShapeDtypeStruct((seqs, width), BF16),
        ),
        in_specs=[in_vmem()] * 3,
        out_specs=(in_hbm(), in_vmem()),
        scratch_shapes=[
            pltpu.VMEM(state.shape, F32),
            pltpu.VMEM((rows, 4 * rows, 2 * dk), BF16),
            dma((parts_of, n_heads)),
        ],
        compiler_params=pltpu.CompilerParams(vmem_limit_bytes=44 * 2**20),
        name="update",
    )(fkv, held, part)
    return layer_out, updated


def solution(mesh):
    in_specs = (
        P(None, ("kv", "tp")),
        P("kv"),
        P("kv", "tp"),
        P("kv", "tp"),
        P("kv", "tp"),
        P("kv", "tp"),
        P("tp"),
        P("kv", "tp", None, None),
        P(),
        P("tp", "kv"),
        P("kv"),
        P("kv", "tp"),
        P("kv", "tp"),
        P("tp", "kv"),
    )
    out_specs = (P(None, ("kv", "tp")), P("kv", "tp", None, None))
    return jax.shard_map(
        functools.partial(body, mesh.shape["kv"], mesh.shape["tp"]),
        mesh=mesh, in_specs=in_specs, out_specs=out_specs, check_vma=False,
    )
```

time: 77.3 us -> 62.5 us (0.81)
  Pallas kernels: 74.7 us -> 61.7 us
  local copies, waits for them, and re-layouts: 1.38 us -> 0.01 us
    pallas_call x3 -> x2, Pallas kernels: 74.7 us -> 61.7 us  [the longest x1 56.1 us: body(): pl.pallas_call(functools.partial(layer_kernel, n_kv, n_tp, features, part...]
    unnamed x1 -> x4, local copies, waits for them, and re-layouts: 1.38 us -> 0.01 us
where the time goes in v1:
time: 62.5 us; the launch traced here: 62.4 us
  Pallas kernels  61.7 us (99%)
  between operations  0.68 us (1%)
    pallas_call x1, Pallas kernels, body(): pl.pallas_call(functools.partial(layer_kernel, n_kv, n_tp, features, part...  56.1 us
    pallas_call x1, Pallas kernels, body(): pl.pallas_call(functools.partial(update_kernel, parts_of, n_kv), out_shap...  5.54 us

profile of v1, /device:TPU:0, one launch (start us, length us, event | category | flops | bytes accessed | tf_op | source)
XLA Modules:
  0.0 62.4 jit_solution(17461189599078936062)
XLA Ops:
  0.6 0.0 slice-start
  0.6 0.0 slice-start.1
  0.7 56.1 %layer.1 = (bf16[2,64,128]{2,1,0:T(8,128)(2,1)S(1)}, f32[3,2,4,16,128]{4,3,2,1,0:T(8,128)S(1)}) custom-call(bf16[128,128]{1,0:T(8,128)(2,1)} %x_hbm.1, f32[1,1024]{1,0:T(1,128)} %bitcast.10, f32[1,1024]{1,0:T(1,128)} %bitcast.11, f32[1,512]{1,0:T(1,128)} %bitcast.12, f32[1,128]{1,0:T(1,128)} %bitcast.13, bf16[1024,512]{1,0:T(8,128)(2,1)} %wq.1, ...), custom_call_target="tpu_custom_call" | custom-call | tf_op jit(solution)/shard_map/layer/pallas_call | solution.py:433
  56.8 0.0 slice-done
  56.8 0.0 slice-done.1
  56.8 5.5 %update.1 = (f32[32,4,128,128]{3,2,1,0:T(8,128)}, bf16[128,128]{1,0:T(8,128)(2,1)}) custom-call(f32[3,2,4,16,128]{4,3,2,1,0:T(8,128)S(1)} %get-tuple-element.6.fkv_ref, f32[32,4,128,128]{3,2,1,0:T(8,128)S(1)} %bitcast.7, bf16[2,64,128]{2,1,0:T(8,128)(2,1)S(1)} %get-tuple-element.7.part_ref), custom_call_target="tpu_custom_call" | custom-call | tf_op jit(solution)/shard_map/update/pallas_call | solution.py:488
  (1 shorter events, 0.0 us)
Async XLA Ops:
  0.6 56.2 %slice-start = ((s8[8388608]{0:T(1024)(128)(4,1)}), s8[4194304]{0:T(1024)(128)(4,1)S(1)}, s32[]{:S(2)}) async-start(s8[8388608]{0:T(1024)(128)(4,1)} %bitcast.6), calls=%async_computation | async-start | bytes 8388608
  0.6 56.2 %slice-start.1 = ((s8[8388608]{0:T(1024)(128)(4,1)}), s8[4194304]{0:T(1024)(128)(4,1)S(1)}, s32[]{:S(2)}) async-start(s8[8388608]{0:T(1024)(128)(4,1)} %bitcast.6), calls=%async_computation.1 | async-start | bytes 8388608

commit v2 on v1

v2 whole, which is shorter than its diff:
```python
import functools

import jax
import jax.numpy as jnp
from jax import lax
from jax.experimental import pallas as pl
from jax.experimental.pallas import tpu as pltpu
from jax.sharding import PartitionSpec as P

EPS = 1e-06
F32 = jnp.float32
BF16 = jnp.bfloat16
LANES = 128


def ring(axis, size):
    me = lax.axis_index(axis)
    return me, [lax.rem(me + step, size) for step in range(1, size)]


def greet(axes):
    barrier = pltpu.get_barrier_semaphore()
    count = 0
    for axis, peers in axes:
        for peer in peers:
            pl.semaphore_signal(
                barrier, inc=1, device_id={axis: peer}, device_id_type=pl.DeviceIdType.MESH
            )
            count += 1
    pl.semaphore_wait(barrier, count)


def remote(source, target, send_sem, recv_sem, axis, peer):
    return pltpu.make_async_remote_copy(
        src_ref=source,
        dst_ref=target,
        send_sem=send_sem,
        recv_sem=recv_sem,
        device_id={axis: peer},
        device_id_type=pl.DeviceIdType.MESH,
    )


def pairs(n_tp):
    me = lax.axis_index("tp")
    core = lax.rem(me, 2)
    return me, core, lax.div(me, 2), me + 1 - 2 * core, n_tp // 2


def landed(ref, sem):
    pltpu.make_async_copy(ref, ref, sem).wait()


def start_gather(n_tp, source, blocks, send, recv):
    me, _, _, partner, half = pairs(n_tp)
    targets = [lax.rem(me + 2 * i, n_tp) for i in range(1, half)] + [partner]
    direct = [
        remote(source, blocks.at[me], send, recv.at[i], "tp", target)
        for i, target in enumerate(targets)
    ]
    for copy in direct:
        copy.start()
    blocks[pl.ds(me, 1)] = source[...][None]
    return direct


def relay_gather(n_tp, blocks, direct, send, recv):
    me, _, _, partner, half = pairs(n_tp)
    for i in range(1, half):
        origin = lax.rem(me - 2 * i + n_tp, n_tp)
        direct[i - 1].wait_recv()
        remote(
            blocks.at[origin], blocks.at[origin], send, recv.at[half - 1], "tp", partner
        ).start()


def end_gather(n_tp, blocks, recv):
    half = n_tp // 2
    landed(blocks.at[pl.ds(0, half)], recv.at[half - 1])


def scale_block(blocks, gain_ref, scaled, count, width):
    squares = None
    for j in range(count):
        rows = blocks[j].astype(F32)
        cols = slice(j * width, (j + 1) * width)
        scaled[:, cols] = (rows * gain_ref[:, cols]).astype(BF16)
        term = rows * rows
        squares = term if squares is None else squares + term
    total = jnp.sum(squares, axis=1, keepdims=True)
    return jnp.broadcast_to(total, (total.shape[0], LANES))


def split(value):
    high = value.astype(BF16).astype(F32)
    return high, value - high


def layer_kernel(
    n_kv, n_tp, features, parts_of,
    x_hbm, gain_a_hbm, gain_b_hbm, bound_hbm, head_gain_hbm,
    wq, wf, wi, wo, state_hbm, w_mix, w_gate, w_up, w_down,
    out_ref, state,
    xs, gain_a, gain_b, bound, head_gain, proj_w, state16, picks, fkv, mix_w, gate_w, down_w,
    blocks, scaled, squares, squares_in, raws, raws_in, normed, heads_all,
    sums, pair_in, joined, sums_in, mixed,
    parts, parts_in, hidden, hiddens,
    x_sem, small_sem, proj_sem, state_sem, w_sem,
    g_send, g_recv, q_send, q_recv, r_send, r_recv, n_send, n_recv,
    t_send, t_recv, p_send, p_recv, h_send, h_recv,
):
    halves = range(parts_of)
    _, seqs, width = xs.shape
    rows = seqs // n_kv
    n_heads, depth, wide = proj_w.shape
    dk = wide // 4
    units = gate_w.shape[1]
    half = n_tp // 2

    x_loads = []
    for h in halves:
        for o in range(n_kv):
            x_loads.append(pltpu.make_async_copy(
                x_hbm.at[pl.ds((o * parts_of + h) * rows, rows), :],
                xs.at[h, pl.ds(o * rows, rows), :], x_sem.at[h],
            ))
    small_loads = [
        pltpu.make_async_copy(source, target, small_sem.at[i])
        for i, (source, target) in enumerate((
            (gain_a_hbm, gain_a), (gain_b_hbm, gain_b), (bound_hbm, bound), (head_gain_hbm, head_gain),
        ))
    ]
    proj_loads = [
        [
            pltpu.make_async_copy(
                source.at[:, pl.ds(j * dk, dk)], proj_w.at[j, :, pl.ds(p * dk, dk)], proj_sem.at[j]
            )
            for p, source in enumerate((wq, wf, wi, wo))
        ]
        for j in range(n_heads)
    ]
    state_loads = [
        pltpu.make_async_copy(
            state_hbm.at[pl.ds(h * rows, rows)], state.at[pl.ds(h * rows, rows)], state_sem.at[h]
        )
        for h in halves
    ]
    w_loads = [
        pltpu.make_async_copy(source, target, w_sem.at[i])
        for i, (source, target) in enumerate(
            ((w_mix, mix_w), (w_gate, gate_w.at[0]), (w_up, gate_w.at[1]), (w_down, down_w))
        )
    ]
    for load in x_loads + small_loads + sum(proj_loads, []):
        load.start()

    kv, kv_peers = ring("kv", n_kv)
    me, core, chip, partner, _ = pairs(n_tp)
    own = pl.ds(pl.multiple_of(kv * rows, rows), rows)
    peer_rows = [pl.ds(pl.multiple_of(peer * rows, rows), rows) for peer in kv_peers]
    tp_peers = ring("tp", n_tp)[1]
    greet((("kv", kv_peers), ("tp", [partner] + tp_peers[1::2])))

    def send_squares(h, stage):
        for i, peer in enumerate(kv_peers):
            remote(
                squares.at[stage, h, peer_rows[i], :], squares_in.at[stage, h, i],
                q_send, q_recv.at[stage, h], "kv", peer,
            ).start()

    def inverse_of(h, stage):
        landed(squares_in.at[stage, h], q_recv.at[stage, h])
        total = squares[stage, h, own, :]
        for i in range(n_kv - 1):
            total = total + squares_in[stage, h, i]
        return lax.rsqrt(total[:, :1] / features + EPS)

    def spread(h, source, target, send, recv):
        for peer in kv_peers:
            remote(source, target.at[h, own, :], send, recv.at[h], "kv", peer).start()
        target[h, own, :] = source[...]

    def others(target):
        return target.at[pl.ds(0, (n_kv - 1) * rows), :]

    group = max(1, 256 // width)
    while n_tp % group:
        group -= 1

    def start_reduce(h, stage, left, weight):
        for t in range(0, n_tp, group):
            part = jnp.dot(
                left[...], weight[:, t * width : (t + group) * width], preferred_element_type=F32
            ).astype(BF16)
            for j in range(group):
                sums[stage, h, (t + j) % 2, (t + j) // 2] = part[:, j * width : (j + 1) * width]
        first = remote(
            sums.at[stage, h, 1 - core], pair_in.at[stage, h],
            t_send.at[0], t_recv.at[stage, h, 0], "tp", partner,
        )
        first.start()
        return first

    def pair_sum(h, stage, place):
        mine = sums[stage, h, pl.ds(core, 1), pl.ds(place, 1)][0, 0].astype(F32)
        return mine + pair_in[stage, h, pl.ds(place, 1)][0].astype(F32)

    def join_reduce(h, stage, first):
        first.wait_recv()
        for i in range(1, half):
            joined[stage, h, i - 1] = pair_sum(h, stage, lax.rem(chip + i, half)).astype(BF16)
            remote(
                joined.at[stage, h, i - 1], sums_in.at[stage, h, i - 1],
                t_send.at[1], t_recv.at[stage, h, 1], "tp", lax.rem(me + 2 * i, n_tp),
            ).start()

    def end_reduce(h, stage, base):
        total = base + pair_sum(h, stage, chip)
        landed(sums_in.at[stage, h], t_recv.at[stage, h, 1])
        for i in range(half - 1):
            total = total + sums_in[stage, h, i].astype(F32)
        return total.astype(BF16)

    direct = {}

    for h in halves:
        landed(xs.at[h], x_sem.at[h])
        direct[h] = start_gather(n_tp, xs.at[h], blocks.at[0, h], g_send.at[0], g_recv.at[0, h])
    place = lax.broadcasted_iota(jnp.int32, (4 * rows, 2 * dk), 0)
    lane = lax.broadcasted_iota(jnp.int32, (4 * rows, 2 * dk), 1)
    side = jnp.where((place < 2 * rows) == (lane < dk), 1.0, 0.0)
    owner = lax.rem(place, rows)
    for s in range(rows):
        picks[s] = jnp.where(owner == s, side, 0.0).astype(BF16)

    def update(h):
        def step(j, carry):
            left = jnp.concatenate(
                [*split(fkv[0, h, j]), *split(fkv[1, h, j])], axis=0
            ).T.astype(BF16)
            value = fkv[2, h, j]
            for s in range(rows):
                wide = jnp.dot(left, picks[s], preferred_element_type=F32)
                state[h * rows + s, j] = (
                    wide[:, :dk] * state[h * rows + s, j] + wide[:, dk:] * value[s : s + 1, :]
                )
            return carry
        lax.fori_loop(0, n_heads, step, 0)

    for load in small_loads:
        load.wait()
    for h in halves:
        relay_gather(n_tp, blocks.at[0, h], direct[h], g_send.at[0], g_recv.at[0, h])
    for load in state_loads:
        load.start()
    for h in halves:
        end_gather(n_tp, blocks.at[0, h], g_recv.at[0, h])
        squares[0, h] = scale_block(blocks.at[0, h], gain_a, scaled.at[0, h], n_tp, width)
        send_squares(h, 0)
        for j in range(n_heads):
            if h == 0:
                landed(proj_w.at[j], proj_sem.at[j])
            raws[h, j] = jnp.dot(scaled[0, h], proj_w[j], preferred_element_type=F32).astype(BF16)
            for i, peer in enumerate(kv_peers):
                remote(
                    raws.at[h, j, peer_rows[i], :], raws_in.at[h, j, i],
                    r_send, r_recv.at[h, j], "kv", peer,
                ).start()

    for load in w_loads:
        load.start()

    def narrow(h):
        def step(j, carry):
            for s in range(rows):
                state16[h, j, :, s * dk : (s + 1) * dk] = state[h * rows + s, j].astype(BF16)
            return carry
        lax.fori_loop(0, n_heads, step, 0)

    for h in halves:
        state_loads[h].wait()
        narrow(h)
    spots = lax.broadcasted_iota(jnp.int32, (rows, dk), 0)
    for h in halves:
        inverse = inverse_of(h, 0)
        for j in range(n_heads):
            cols = slice(j * dk, (j + 1) * dk)
            total = raws[h, j, own, :].astype(F32)
            landed(raws_in.at[h, j], r_recv.at[h, j])
            for i in range(n_kv - 1):
                total = total + raws_in[h, j, i].astype(F32)
            total = total * inverse
            query, raw, value, gate = (total[:, p * dk : (p + 1) * dk] for p in range(4))
            low = bound[:, cols]
            forget = low + (1.0 - low) * jax.nn.sigmoid(raw)
            keyvec = (1.0 - low) * jax.nn.sigmoid(-raw)
            query = query * jax.nn.sigmoid(query)
            fkv[0, h, j] = forget
            fkv[1, h, j] = keyvec
            fkv[2, h, j] = value
            left = (query * forget).astype(BF16)
            head = jnp.sum(query * keyvec, axis=1, keepdims=True) * value
            seen = jnp.dot(left, state16[h, j], preferred_element_type=F32)
            for s in range(rows):
                head = head + jnp.where(spots == s, seen[:, s * dk : (s + 1) * dk], 0.0)
            scale = lax.rsqrt(jnp.mean(head * head, axis=1, keepdims=True) + EPS)
            normed[h, :, cols] = (
                head * scale * head_gain[...] * (gate * jax.nn.sigmoid(gate))
            ).astype(BF16)
        spread(h, normed.at[h], heads_all, n_send, n_recv)

    w_loads[0].wait()
    for h in halves:
        landed(others(heads_all.at[h]), n_recv.at[h])
        join_reduce(h, 0, start_reduce(h, 0, heads_all.at[h], mix_w))
    for h in halves:
        mixed[h] = end_reduce(h, 0, xs[h].astype(F32))
        direct[h] = start_gather(n_tp, mixed.at[h], blocks.at[1, h], g_send.at[1], g_recv.at[1, h])
        if h == 0:
            update(0)

    def relay(h):
        relay_gather(n_tp, blocks.at[1, h], direct[h], g_send.at[1], g_recv.at[1, h])

    relay(0)
    step = min(512, units)
    chunks = [(c, min(c + step, units)) for c in range(0, units, step)]
    for h in halves:
        end_gather(n_tp, blocks.at[1, h], g_recv.at[1, h])
        squares[1, h] = scale_block(blocks.at[1, h], gain_b, scaled.at[1, h], n_tp, width)
        send_squares(h, 1)
        for k, (c, end) in enumerate(chunks):
            for g in range(2):
                if h == 0 and k == 0:
                    w_loads[1 + g].wait()
                parts[h, g, :, c:end] = lax.dot_general(
                    scaled[1, h], gate_w[g, c:end, :], (((1,), (1,)), ((), ())),
                    preferred_element_type=F32,
                ).astype(BF16)
                for i, peer in enumerate(kv_peers):
                    remote(
                        parts.at[h, g, peer_rows[i], c:end], parts_in.at[h, i, g, :, c:end],
                        p_send, p_recv.at[h], "kv", peer,
                    ).start()
            if k == len(chunks) // 2 and h + 1 < parts_of:
                relay(h + 1)
    for h in range(1, parts_of):
        update(h)
    for h in halves:
        inverse = inverse_of(h, 1)
        landed(parts_in.at[h], p_recv.at[h])
        both = []
        for g in range(2):
            total = parts[h, g, own, :].astype(F32)
            for i in range(n_kv - 1):
                total = total + parts_in[h, i, g].astype(F32)
            both.append(total * inverse)
        hidden[h] = (both[0] * jax.nn.sigmoid(both[0]) * both[1]).astype(BF16)
        if h == 0:
            landed(parts_in, p_send)
        spread(h, hidden.at[h], hiddens, h_send, h_recv)
    w_loads[3].wait()
    for h in halves:
        landed(others(hiddens.at[h]), h_recv.at[h])
        join_reduce(h, 1, start_reduce(h, 1, hiddens.at[h], down_w))
    for h in halves:
        out_ref[h] = end_reduce(h, 1, mixed[h].astype(F32))
    for stage in range(2):
        landed(blocks.at[stage, :, pl.ds(0, n_tp - 1)], g_send.at[stage])
    for ref, sem in (
        (squares_in, q_send), (raws_in, r_send), (pair_in, t_send.at[0]), (sums_in, t_send.at[1]),
        (heads_all.at[:, pl.ds(0, (n_kv - 1) * rows)], n_send),
        (hiddens.at[:, pl.ds(0, (n_kv - 1) * rows)], h_send),
    ):
        landed(ref, sem)


def deliver_kernel(parts_of, n_kv, state_ref, part_ref, new_ref, out_ref, sems):
    local = state_ref.shape[0]
    rows = local // parts_of
    count = sems.shape[0]
    some = local // count
    copies = [
        pltpu.make_async_copy(
            state_ref.at[pl.ds(i * some, some)], new_ref.at[pl.ds(i * some, some)], sems.at[i]
        )
        for i in range(count)
    ]
    for copy in copies:
        copy.start()
    for h in range(parts_of):
        for o in range(n_kv):
            out_ref[pl.ds((o * parts_of + h) * rows, rows), :] = part_ref[h, pl.ds(o * rows, rows), :]
    for copy in copies:
        copy.wait()


def in_vmem():
    return pl.BlockSpec(memory_space=pltpu.VMEM)


def in_hbm():
    return pl.BlockSpec(memory_space=pltpu.HBM)


def body(
    n_kv, n_tp,
    residual, mixer_gain, w_query, w_forget, w_input, w_outgate, lower_bound, state,
    head_gain, w_mix_out, ffn_gain, w_gate, w_up, w_down,
):
    seqs, width = residual.shape
    depth, hid = w_query.shape
    local, n_heads, dk, dv = state.shape
    units = w_gate.shape[1]
    features = depth * n_kv
    half = n_tp // 2
    parts_of = 2 if local % 32 == 0 else 1
    rows = local // parts_of
    some = seqs // parts_of
    dma = pltpu.SemaphoreType.DMA
    stay = lambda array: pltpu.with_memory_space_constraint(array, pltpu.HBM)

    part, held = pl.pallas_call(
        functools.partial(layer_kernel, n_kv, n_tp, features, parts_of),
        out_shape=(
            jax.ShapeDtypeStruct((parts_of, some, width), BF16),
            jax.ShapeDtypeStruct(state.shape, F32),
        ),
        in_specs=[in_hbm()] * 14,
        out_specs=(in_vmem(), in_vmem()),
        scratch_shapes=[
            pltpu.VMEM((parts_of, some, width), BF16),
            pltpu.VMEM((1, depth), F32),
            pltpu.VMEM((1, depth), F32),
            pltpu.VMEM((1, hid), F32),
            pltpu.VMEM((1, dv), F32),
            pltpu.VMEM((n_heads, depth, 4 * dk), BF16),
            pltpu.VMEM((parts_of, n_heads, dk, rows * dv), BF16),
            pltpu.VMEM((rows, 4 * rows, 2 * dk), BF16),
            pltpu.VMEM((3, parts_of, n_heads, rows, dk), F32),
            pltpu.VMEM(w_mix_out.shape, BF16),
            pltpu.VMEM((2, units, depth), BF16),
            pltpu.VMEM(w_down.shape, BF16),
            pltpu.VMEM((2, parts_of, n_tp, some, width), BF16),
            pltpu.VMEM((2, parts_of, some, depth), BF16),
            pltpu.VMEM((2, parts_of, some, LANES), F32),
            pltpu.VMEM((2, parts_of, n_kv - 1, rows, LANES), F32),
            pltpu.VMEM((parts_of, n_heads, some, 4 * dk), BF16),
            pltpu.VMEM((parts_of, n_heads, n_kv - 1, rows, 4 * dk), BF16),
            pltpu.VMEM((parts_of, rows, hid), BF16),
            pltpu.VMEM((parts_of, some, hid), BF16),
            pltpu.VMEM((2, parts_of, 2, half, some, width), BF16),
            pltpu.VMEM((2, parts_of, half, some, width), BF16),
            pltpu.VMEM((2, parts_of, half - 1, some, width), BF16),
            pltpu.VMEM((2, parts_of, half - 1, some, width), BF16),
            pltpu.VMEM((parts_of, some, width), BF16),
            pltpu.VMEM((parts_of, 2, some, units), BF16),
            pltpu.VMEM((parts_of, n_kv - 1, 2, rows, units), BF16),
            pltpu.VMEM((parts_of, rows, units), BF16),
            pltpu.VMEM((parts_of, some, units), BF16),
            dma((parts_of,)), dma((4,)), dma((n_heads,)), dma((parts_of,)), dma((4,)),
            dma((2,)), dma((2, parts_of, half)),
            dma, dma((2, parts_of)),
            dma, dma((parts_of, n_heads)),
            dma, dma((parts_of,)),
            dma((2,)), dma((2, parts_of, 2)),
            dma, dma((parts_of,)),
            dma, dma((parts_of,)),
        ],
        compiler_params=pltpu.CompilerParams(
            collective_id=0, has_side_effects=True, vmem_limit_bytes=44 * 2**20
        ),
        name="layer",
    )(*map(stay, (
        residual, mixer_gain.reshape(1, depth), ffn_gain.reshape(1, depth),
        lower_bound.reshape(1, hid), head_gain.reshape(1, dv),
        w_query, w_forget, w_input, w_outgate, state, w_mix_out, w_gate.T, w_up.T, w_down,
    )))

    held = pltpu.with_memory_space_constraint(held, pltpu.VMEM)
    updated, layer_out = pl.pallas_call(
        functools.partial(deliver_kernel, parts_of, n_kv),
        out_shape=(
            jax.ShapeDtypeStruct(state.shape, F32),
            jax.ShapeDtypeStruct((seqs, width), BF16),
        ),
        in_specs=[in_vmem()] * 2,
        out_specs=(in_hbm(), in_vmem()),
        scratch_shapes=[dma((8 if local % 8 == 0 else 1,))],
        compiler_params=pltpu.CompilerParams(vmem_limit_bytes=16 * 2**20),
        name="deliver",
    )(held, part)
    return layer_out, updated


def solution(mesh):
    in_specs = (
        P(None, ("kv", "tp")),
        P("kv"),
        P("kv", "tp"),
        P("kv", "tp"),
        P("kv", "tp"),
        P("kv", "tp"),
        P("tp"),
        P("kv", "tp", None, None),
        P(),
        P("tp", "kv"),
        P("kv"),
        P("kv", "tp"),
        P("kv", "tp"),
        P("tp", "kv"),
    )
    out_specs = (P(None, ("kv", "tp")), P("kv", "tp", None, None))
    return jax.shard_map(
        functools.partial(body, mesh.shape["kv"], mesh.shape["tp"]),
        mesh=mesh, in_specs=in_specs, out_specs=out_specs, check_vma=False,
    )
```

time: 62.5 us -> 55.6 us (0.89)
  Pallas kernels: 61.7 us -> 54.9 us
    pallas_call x1, Pallas kernels: 56.1 us -> 50.9 us  [body(): pl.pallas_call(functools.partial(layer_kernel, n_kv, n_tp, features, part...]
    pallas_call x1, Pallas kernels: 5.54 us -> 3.98 us  [body(): pl.pallas_call(functools.partial(deliver_kernel, parts_of, n_kv), out_sha...]
where the time goes in v2:
time: 55.6 us; the launch traced here: 55.5 us
  Pallas kernels  54.9 us (99%)
  between operations  0.64 us (1%)
    pallas_call x1, Pallas kernels, body(): pl.pallas_call(functools.partial(layer_kernel, n_kv, n_tp, features, part...  50.9 us
    pallas_call x1, Pallas kernels, body(): pl.pallas_call(functools.partial(deliver_kernel, parts_of, n_kv), out_sha...  3.98 us

profile of v2, /device:TPU:0, one launch (start us, length us, event | category | flops | bytes accessed | tf_op | source)
XLA Modules:
  0.0 55.5 jit_solution(10836302615123687359)
XLA Ops:
  0.6 50.9 %layer.1 = (bf16[2,64,128]{2,1,0:T(8,128)(2,1)S(1)}, f32[32,4,128,128]{3,2,1,0:T(8,128)S(1)}) custom-call(bf16[128,128]{1,0:T(8,128)(2,1)} %x_hbm.1, f32[1,1024]{1,0:T(1,128)} %bitcast.8, f32[1,1024]{1,0:T(1,128)} %bitcast.9, f32[1,512]{1,0:T(1,128)} %bitcast.10, f32[1,128]{1,0:T(1,128)} %bitcast.11, bf16[1024,512]{1,0:T(8,128)(2,1)} %wq.1, ...), custom_call_target="tpu_custom_call" | custom-call | tf_op jit(solution)/shard_map/layer/pallas_call | solution.py:423
  51.5 4.0 %deliver.1 = (f32[32,4,128,128]{3,2,1,0:T(8,128)}, bf16[128,128]{1,0:T(8,128)(2,1)}) custom-call(f32[32,4,128,128]{3,2,1,0:T(8,128)S(1)} %get-tuple-element.6.state_ref, bf16[2,64,128]{2,1,0:T(8,128)(2,1)S(1)} %get-tuple-element.7.part_ref), custom_call_target="tpu_custom_call" | custom-call | tf_op jit(solution)/shard_map/deliver/pallas_call | solution.py:481

commit v3 on v2

--- a/solution.py
+++ b/solution.py
@@ -79,7 +79,7 @@
     landed(blocks.at[pl.ds(0, half)], recv.at[half - 1])
 
 
-def scale_block(blocks, gain_ref, scaled, count, width):
+def scale_block(blocks, gain_ref, scaled, count, width, owners):
     squares = None
     for j in range(count):
         rows = blocks[j].astype(F32)
@@ -88,7 +88,15 @@
         term = rows * rows
         squares = term if squares is None else squares + term
     total = jnp.sum(squares, axis=1, keepdims=True)
-    return jnp.broadcast_to(total, (total.shape[0], LANES))
+    rows = total.shape[0] // owners
+    lane = lax.broadcasted_iota(jnp.int32, (rows, LANES), 1)
+    spot = lax.broadcasted_iota(jnp.int32, (rows, LANES), 0)
+    return [
+        jnp.sum(
+            jnp.where(lane == spot, total[o * rows : (o + 1) * rows], 0.0), axis=0, keepdims=True
+        )
+        for o in range(owners)
+    ]
 
 
 def split(value):
@@ -162,18 +170,26 @@
     greet((("kv", kv_peers), ("tp", [partner] + tp_peers[1::2])))
 
     def send_squares(h, stage):
+        sums_of = scale_block(
+            blocks.at[stage, h], (gain_a, gain_b)[stage], scaled.at[stage, h], n_tp, width, n_kv
+        )
+        for o in range(n_kv):
+            squares[stage, h, o] = sums_of[o]
         for i, peer in enumerate(kv_peers):
             remote(
-                squares.at[stage, h, peer_rows[i], :], squares_in.at[stage, h, i],
+                squares.at[stage, h, peer], squares_in.at[stage, h, i],
                 q_send, q_recv.at[stage, h], "kv", peer,
             ).start()
 
     def inverse_of(h, stage):
         landed(squares_in.at[stage, h], q_recv.at[stage, h])
-        total = squares[stage, h, own, :]
+        total = squares[stage, h, pl.ds(kv, 1)][0]
         for i in range(n_kv - 1):
             total = total + squares_in[stage, h, i]
-        return lax.rsqrt(total[:, :1] / features + EPS)
+        lane = lax.broadcasted_iota(jnp.int32, (rows, LANES), 1)
+        spot = lax.broadcasted_iota(jnp.int32, (rows, LANES), 0)
+        total = jnp.sum(jnp.where(lane == spot, total, 0.0), axis=1, keepdims=True)
+        return lax.rsqrt(total / features + EPS)
 
     def spread(h, source, target, send, recv):
         for peer in kv_peers:
@@ -221,7 +237,7 @@
             total = total + sums_in[stage, h, i].astype(F32)
         return total.astype(BF16)
 
-    direct = {}
+    direct, firsts = {}, {}
 
     for h in halves:
         landed(xs.at[h], x_sem.at[h])
@@ -255,7 +271,6 @@
         load.start()
     for h in halves:
         end_gather(n_tp, blocks.at[0, h], g_recv.at[0, h])
-        squares[0, h] = scale_block(blocks.at[0, h], gain_a, scaled.at[0, h], n_tp, width)
         send_squares(h, 0)
         for j in range(n_heads):
             if h == 0:
@@ -324,10 +339,10 @@
 
     relay(0)
     step = min(512, units)
-    chunks = [(c, min(c + step, units)) for c in range(0, units, step)]
+    edges = [0, *range(step // 2, units - step // 2, step), units]
+    chunks = list(zip(edges[:-1], edges[1:]))
     for h in halves:
         end_gather(n_tp, blocks.at[1, h], g_recv.at[1, h])
-        squares[1, h] = scale_block(blocks.at[1, h], gain_b, scaled.at[1, h], n_tp, width)
         send_squares(h, 1)
         for k, (c, end) in enumerate(chunks):
             for g in range(2):
@@ -342,7 +357,7 @@
                         parts.at[h, g, peer_rows[i], c:end], parts_in.at[h, i, g, :, c:end],
                         p_send, p_recv.at[h], "kv", peer,
                     ).start()
-            if k == len(chunks) // 2 and h + 1 < parts_of:
+            if k == 1 and h + 1 < parts_of:
                 relay(h + 1)
     for h in range(1, parts_of):
         update(h)
@@ -356,19 +371,19 @@
                 total = total + parts_in[h, i, g].astype(F32)
             both.append(total * inverse)
         hidden[h] = (both[0] * jax.nn.sigmoid(both[0]) * both[1]).astype(BF16)
-        if h == 0:
-            landed(parts_in, p_send)
         spread(h, hidden.at[h], hiddens, h_send, h_recv)
     w_loads[3].wait()
     for h in halves:
         landed(others(hiddens.at[h]), h_recv.at[h])
-        join_reduce(h, 1, start_reduce(h, 1, hiddens.at[h], down_w))
+        firsts[h] = start_reduce(h, 1, hiddens.at[h], down_w)
+    for h in halves:
+        join_reduce(h, 1, firsts[h])
     for h in halves:
         out_ref[h] = end_reduce(h, 1, mixed[h].astype(F32))
     for stage in range(2):
         landed(blocks.at[stage, :, pl.ds(0, n_tp - 1)], g_send.at[stage])
     for ref, sem in (
-        (squares_in, q_send), (raws_in, r_send), (pair_in, t_send.at[0]), (sums_in, t_send.at[1]),
+        (squares_in, q_send), (raws_in, r_send), (parts_in, p_send), (pair_in, t_send.at[0]), (sums_in, t_send.at[1]),
         (heads_all.at[:, pl.ds(0, (n_kv - 1) * rows)], n_send),
         (hiddens.at[:, pl.ds(0, (n_kv - 1) * rows)], h_send),
     ):
@@ -443,8 +458,8 @@
             pltpu.VMEM(w_down.shape, BF16),
             pltpu.VMEM((2, parts_of, n_tp, some, width), BF16),
             pltpu.VMEM((2, parts_of, some, depth), BF16),
-            pltpu.VMEM((2, parts_of, some, LANES), F32),
-            pltpu.VMEM((2, parts_of, n_kv - 1, rows, LANES), F32),
+            pltpu.VMEM((2, parts_of, n_kv, 1, LANES), F32),
+            pltpu.VMEM((2, parts_of, n_kv - 1, 1, LANES), F32),
             pltpu.VMEM((parts_of, n_heads, some, 4 * dk), BF16),
             pltpu.VMEM((parts_of, n_heads, n_kv - 1, rows, 4 * dk), BF16),
             pltpu.VMEM((parts_of, rows, hid), BF16),

time: 55.6 us -> 54.5 us (0.980)
  Pallas kernels: 54.9 us -> 53.7 us
    pallas_call x1, Pallas kernels: 50.9 us -> 49.7 us  [body(): pl.pallas_call(functools.partial(layer_kernel, n_kv, n_tp, features, part...]
where the time goes in v3:
time: 54.5 us; the launch traced here: 54.4 us
  Pallas kernels  53.7 us (99%)
  between operations  0.64 us (1%)
    pallas_call x1, Pallas kernels, body(): pl.pallas_call(functools.partial(layer_kernel, n_kv, n_tp, features, part...  49.7 us
    pallas_call x1, Pallas kernels, body(): pl.pallas_call(functools.partial(deliver_kernel, parts_of, n_kv), out_sha...  3.98 us

profile of v3, /device:TPU:0, one launch (start us, length us, event | category | flops | bytes accessed | tf_op | source)
XLA Modules:
  0.0 54.4 jit_solution(9837599719711418448)
XLA Ops:
  0.6 49.7 %layer.1 = (bf16[2,64,128]{2,1,0:T(8,128)(2,1)S(1)}, f32[32,4,128,128]{3,2,1,0:T(8,128)S(1)}) custom-call(bf16[128,128]{1,0:T(8,128)(2,1)} %x_hbm.1, f32[1,1024]{1,0:T(1,128)} %bitcast.8, f32[1,1024]{1,0:T(1,128)} %bitcast.9, f32[1,512]{1,0:T(1,128)} %bitcast.10, f32[1,128]{1,0:T(1,128)} %bitcast.11, bf16[1024,512]{1,0:T(8,128)(2,1)} %wq.1, ...), custom_call_target="tpu_custom_call" | custom-call | tf_op jit(solution)/shard_map/layer/pallas_call | solution.py:438
  50.4 4.0 %deliver.1 = (f32[32,4,128,128]{3,2,1,0:T(8,128)}, bf16[128,128]{1,0:T(8,128)(2,1)}) custom-call(f32[32,4,128,128]{3,2,1,0:T(8,128)S(1)} %get-tuple-element.6.state_ref, bf16[2,64,128]{2,1,0:T(8,128)(2,1)S(1)} %get-tuple-element.7.part_ref), custom_call_target="tpu_custom_call" | custom-call | tf_op jit(solution)/shard_map/deliver/pallas_call | solution.py:496

commit v4 on v3

--- a/solution.py
+++ b/solution.py
@@ -159,7 +159,7 @@
             ((w_mix, mix_w), (w_gate, gate_w.at[0]), (w_up, gate_w.at[1]), (w_down, down_w))
         )
     ]
-    for load in x_loads + small_loads + sum(proj_loads, []):
+    for load in x_loads + small_loads:
         load.start()
 
     kv, kv_peers = ring("kv", n_kv)
@@ -242,6 +242,8 @@
     for h in halves:
         landed(xs.at[h], x_sem.at[h])
         direct[h] = start_gather(n_tp, xs.at[h], blocks.at[0, h], g_send.at[0], g_recv.at[0, h])
+    for load in sum(proj_loads, []):
+        load.start()
     place = lax.broadcasted_iota(jnp.int32, (4 * rows, 2 * dk), 0)
     lane = lax.broadcasted_iota(jnp.int32, (4 * rows, 2 * dk), 1)
     side = jnp.where((place < 2 * rows) == (lane < dk), 1.0, 0.0)

time: 54.5 us -> 54.5 us (level)
  no operation moved by 1% of the time
where the time goes in v4:
time: 54.5 us; the launch traced here: 54.3 us
  Pallas kernels  53.7 us (99%)
  between operations  0.64 us (1%)
    pallas_call x1, Pallas kernels, body(): pl.pallas_call(functools.partial(layer_kernel, n_kv, n_tp, features, part...  49.7 us
    pallas_call x1, Pallas kernels, body(): pl.pallas_call(functools.partial(deliver_kernel, parts_of, n_kv), out_sha...  3.98 us

profile of v4, /device:TPU:0, one launch (start us, length us, event | category | flops | bytes accessed | tf_op | source)
XLA Modules:
  0.0 54.3 jit_solution(6655630506436812315)
XLA Ops:
  0.6 49.7 %layer.1 = (bf16[2,64,128]{2,1,0:T(8,128)(2,1)S(1)}, f32[32,4,128,128]{3,2,1,0:T(8,128)S(1)}) custom-call(bf16[128,128]{1,0:T(8,128)(2,1)} %x_hbm.1, f32[1,1024]{1,0:T(1,128)} %bitcast.8, f32[1,1024]{1,0:T(1,128)} %bitcast.9, f32[1,512]{1,0:T(1,128)} %bitcast.10, f32[1,128]{1,0:T(1,128)} %bitcast.11, bf16[1024,512]{1,0:T(8,128)(2,1)} %wq.1, ...), custom_call_target="tpu_custom_call" | custom-call | tf_op jit(solution)/shard_map/layer/pallas_call | solution.py:440
  50.3 4.0 %deliver.1 = (f32[32,4,128,128]{3,2,1,0:T(8,128)}, bf16[128,128]{1,0:T(8,128)(2,1)}) custom-call(f32[32,4,128,128]{3,2,1,0:T(8,128)S(1)} %get-tuple-element.6.state_ref, bf16[2,64,128]{2,1,0:T(8,128)(2,1)S(1)} %get-tuple-element.7.part_ref), custom_call_target="tpu_custom_call" | custom-call | tf_op jit(solution)/shard_map/deliver/pallas_call | solution.py:498
